TPU v7x, 32 devices: a whole 2x2x4 slice. The times are simulated.
32 devices in a mesh: sp: 8 (over z, y), dp: 4 (over x, core).
Axes of the slice: x: 2, y: 2, z: 4, core: 2. Of those that a mesh axis runs over, the one named last changes fastest.
Arguments:
- u_pre: bfloat16 [4, 8192, 2048], P('dp', 'sp'), may hold values from -6 to 6
- v_pre: bfloat16 [4, 8192, 2048], P('dp', 'sp'), may hold values from -6 to 6
- d_out: bfloat16 [4, 8192, 2048], P('dp', 'sp'), may hold values from -6 to 6
- w_mix: bfloat16 [16, 128, 128], replicated, may hold values from -0.5 to 0.5
- mix_bias: float32 [16, 128], replicated, may hold values from 0.1 to 1.9
- norm_gain: float32 [16, 128], replicated, may hold values from 0.1 to 1.9
- norm_shift: float32 [16, 128], replicated, may hold values from -3 to 3
- w_out: bfloat16 [2048, 2048], P('dp'), may hold values from -0.125 to 0.125
Outputs:
- grad_u: bfloat16 [4, 8192, 2048], P('dp', 'sp')
- grad_v: bfloat16 [4, 8192, 2048], P('dp', 'sp')
- grad_w_out: float32 [2048, 2048], P('dp')
- grad_w_mix: float32 [16, 128, 128], replicated
- grad_mix_bias: float32 [16, 128], replicated
- grad_gain: float32 [16, 128], replicated
- grad_shift: float32 [16, 128], replicated
All inputs are finite; a program needn't handle non-finite values.
Results may differ from a plain program's by a relative error of at most 0.012.
Values may be sent and summed in bfloat16 or wider, within the bound.
A program may use at most 192 MiB of HBM per device.

v0:
```python
import functools

import jax
import jax.numpy as jnp
from jax import lax
from jax.experimental import pallas as pl
from jax.experimental.pallas import tpu as pltpu
from jax.sharding import PartitionSpec as P

EPS = 1e-05
K0 = 0.7978845608028654
K1 = 0.044715
F32 = jnp.float32
BF16 = jnp.bfloat16


def gelu_parts(a):
    sq = a * a
    t = jnp.tanh(a * (K0 + (K0 * K1) * sq))
    half = 0.5 * (1.0 + t)
    return sq, t, half


def gelu(a):
    _, _, half = gelu_parts(a)
    return a * half


def gelu_both(a):
    sq, t, half = gelu_parts(a)
    slope = half + (0.5 * a) * (1.0 - t * t) * (K0 + (3.0 * K0 * K1) * sq)
    return a * half, slope


def norm_parts(gated):
    centre = gated - jnp.mean(gated, axis=-1, keepdims=True)
    inverse = lax.rsqrt(jnp.mean(centre * centre, axis=-1, keepdims=True) + EPS)
    return centre * inverse, inverse


def mm(a, b, ca, cb):
    return lax.dot_general(a, b, (((ca,), (cb,)), ((), ())), preferred_element_type=F32)


def kernel(
    dims,
    u_hbm, v_hbm, d_hbm, wmix_ref, bias_ref, gain_ref, shift_ref, w_ref,
    gu_hbm, gv_hbm, dw_ref, sm_ref,
    u_ref, v_ref, d_ref, gu_ref, gv_ref, in_s, gu_s, gv_s,
    wfull, part, rcore, rx, ry, rz, ag, gs, got, wl_ref, wlt_ref, acc, sbuf, srecv,
    wown_s, wown_r, wx_s, wx_r, wz_s, wz_r, wy_s, wy_r, wfw_s, wfw_r,
    core_s, core_r, xs_s, xs_r, yr_s, yr_r, zr_s, zr_r, za_s, za_r, ya_s, ya_r,
    s1_s, s1_r, s2_s, s2_r,
):
    n_y, n_z, n_dp, gpc, span, chans, width, rows = dims
    n_sp = n_y * n_z
    pairs = n_dp // 2
    n_dev = n_sp * n_dp
    nb = rows // span
    s = lax.axis_index("sp")
    dpi = lax.axis_index("dp")
    x = dpi // 2
    c = dpi % 2
    y = s % n_y
    z = s // n_y
    zp = z % 2
    other = 1 - c
    mate = {"sp": s, "dp": 2 * x + other}
    part_rows = span // (n_dev // (n_dp * gpc))

    def rc(src, dst, ssem, rsem, dev):
        return pltpu.make_async_remote_copy(
            src_ref=src, dst_ref=dst, send_sem=ssem, recv_sem=rsem,
            device_id=dev, device_id_type=pl.DeviceIdType.MESH,
        )

    def each(lo, hi, fn):
        def body(i, carry):
            fn(i)
            return carry
        lax.fori_loop(lo, hi, body, 0)

    def up(k):
        return (x + k) % pairs

    def down(k):
        return (x + pairs - k) % pairs

    def w_own():
        return rc(w_ref, wfull.at[dpi], wown_s, wown_r, mate)

    def at_y(o):
        return {"sp": z * n_y + (y + o) % n_y, "dp": dpi}

    def at_z(o):
        return {"sp": (z + o) % n_z * n_y + y, "dp": dpi}

    def w_x(k):
        return rc(w_ref.at[y, zp], wfull.at[dpi, y, zp], wx_s.at[k], wx_r.at[k], {"sp": s, "dp": 2 * up(k) + c})

    def w_z(k):
        src = 2 * down(k) + c
        to = {"sp": (z + 1 - 2 * zp) * n_y + y, "dp": dpi}
        return rc(wfull.at[src, y, zp], wfull.at[src, y, zp], wz_s.at[k], wz_r.at[k], to)

    def w_y(k, h, o):
        src = 2 * down(k) + c
        block = wfull.at[src, y, (zp + h) % 2]
        return rc(block, block, wy_s.at[k, (zp + h) % 2, o], wy_r.at[k, (zp + h) % 2, o], at_y(o))

    def w_fw(k):
        src = 2 * down(k) + c
        return rc(wfull.at[src], wfull.at[src], wfw_s.at[k], wfw_r.at[k], mate)

    def gid(xx, cc, q):
        return (2 * xx + cc) * gpc + q

    def t_core(k, q):
        return rc(part.at[gid(up(k), other, q)], rcore.at[k, q], core_s.at[k, q], core_r.at[k, q], mate)

    def t_x(k, q):
        return rc(part.at[gid(up(k), c, q)], rx.at[k, q], xs_s.at[k, q], xs_r.at[k, q], {"sp": s, "dp": 2 * up(k) + c})

    def t_yr(q, o):
        return rc(part.at[gid(x, c, q), (y + o) % n_y], ry.at[q, o], yr_s.at[q, o], yr_r.at[q, o], at_y(o))

    def t_zr(q, o):
        return rc(part.at[gid(x, c, q), y, (z + o) % n_z], rz.at[q, o], zr_s.at[q, o], zr_r.at[q, o], at_z(o))

    def t_za(q, o):
        return rc(ag.at[q, y, z], ag.at[q, y, z], za_s.at[q, o], za_r.at[q, o], at_z(o))

    def t_ya(q, o):
        return rc(ag.at[q, y], ag.at[q, y], ya_s.at[q, o], ya_r.at[q, o], at_y(o))

    me = s * n_dp + dpi

    def t_s1(o):
        to = (me + o) % n_dev
        return rc(sbuf.at[to], srecv.at[o], s1_s.at[o], s1_r.at[o], {"sp": to // n_dp, "dp": to % n_dp})

    def t_s2(o):
        to = (me + o) % n_dev
        return rc(sbuf.at[me], srecv.at[n_dev + me], s2_s.at[o], s2_r.at[o], {"sp": to // n_dp, "dp": to % n_dp})

    row = lax.broadcasted_iota(jnp.int32, (span, span), 0)
    col = lax.broadcasted_iota(jnp.int32, (span, span), 1)
    lower = row >= col

    loads = [
        pltpu.make_async_copy(src, dst, in_s.at[n])
        for n, (src, dst) in enumerate(((v_hbm, v_ref), (u_hbm, u_ref), (d_hbm, d_ref)))
    ]
    for load in loads:
        load.start()
    barrier = pltpu.get_barrier_semaphore()

    def greet(o):
        to = (me + o) % n_dev
        pl.semaphore_signal(
            barrier, inc=1, device_id={"sp": to // n_dp, "dp": to % n_dp},
            device_id_type=pl.DeviceIdType.MESH,
        )
    each(1, n_dev, greet)
    pl.semaphore_wait(barrier, n_dev - 1)
    w_own().start()
    for k in range(1, pairs):
        w_x(k).start()
    wfull[dpi] = w_ref[...]

    def lanes(g):
        return pl.ds(pl.multiple_of(g * chans, chans), chans)

    def forward_group(g, half):
        wl = jnp.where(lower, wmix_ref[g], jnp.zeros((), BF16))
        bias = bias_ref[g]
        gain = gain_ref[g]
        shift = shift_ref[g]
        for b in range(nb):
            at = pl.ds(b * span, span)
            scaled, _ = norm_parts(gelu(v_ref[at, lanes(g)].astype(F32)))
            normed = (scaled * gain + shift).astype(BF16)
            mixed = mm(wl, normed, 1, 0) + bias
            out = (gelu(u_ref[at, lanes(g)].astype(F32)) * mixed).astype(BF16)
            got[pl.ds(pl.multiple_of(half * span, span), span), pl.ds(b * span, span)] = out.T

    def core_sum(k, q):
        t_core(k, q).wait_recv()
        g = gid(up(k), c, q)

        def one(j):
            a, b = j // n_z, j % n_z
            part[g, a, b] = (part[g, a, b].astype(F32) + rcore[k, q, a, b].astype(F32)).astype(BF16)
        each(0, n_sp, one)
        t_x(k, q).start()

    def forward_step(i):
        k = (i // gpc + 1) % pairs
        q = i % gpc
        keep = gid(up(k), c, q)
        give = gid(up(k), other, q)
        each(0, 2, lambda h: forward_group(gid(up(k), (c + h) % 2, q), h))

        def one(j):
            r = mm(got[...], d_ref[:, pl.ds(pl.multiple_of(j * width, width), width)], 1, 0)
            part[keep, j // n_z, j % n_z] = r[:span].astype(BF16)
            part[give, j // n_z, j % n_z] = r[span:].astype(BF16)
        each(0, n_sp, one)
        t_core(k, q).start()
        last = i - 1

        @pl.when((i > 0) & (last < (pairs - 1) * gpc))
        def _():
            core_sum((last // gpc + 1) % pairs, last % gpc)

    n_far = (pairs - 1) * gpc
    for load in loads:
        load.wait()
    each(0, n_far // 2, forward_step)
    for k in range(1, pairs):
        w_x(k).wait_recv()
        w_z(k).start()
        each(1, n_y, lambda o: w_y(k, 0, o).start())
    each(n_far // 2, n_far + 1, forward_step)
    for k in range(1, pairs):
        w_z(k).wait_recv()
        each(1, n_y, lambda o: w_y(k, 1, o).start())
    each(n_far + 1, n_far + gpc, forward_step)
    w_own().wait_recv()

    def forward_w():
        for k in range(1, pairs):
            each(1, n_y, lambda o: w_y(k, 0, o).wait_recv())
            each(1, n_y, lambda o: w_y(k, 1, o).wait_recv())
            w_fw(k).start()

    def yr_start(q):
        t_core(0, q).wait_recv()
        for k in range(1, pairs):
            t_x(k, q).wait_recv()
        g = gid(x, c, q)

        def one(j):
            a, b = j // n_z, j % n_z
            total = part[g, a, b].astype(F32) + rcore[0, q, a, b].astype(F32)
            for k in range(1, pairs):
                total = total + rx[k, q, a, b].astype(F32)
            part[g, a, b] = total.astype(BF16)
        each(0, n_sp, one)
        each(1, n_y, lambda o: t_yr(q, o).start())

    def zr_start(q):
        each(1, n_y, lambda o: t_yr(q, o).wait_recv())
        g = gid(x, c, q)

        def one(b):
            total = part[g, y, b].astype(F32)
            for o in range(1, n_y):
                total = total + ry[q, o, b].astype(F32)
            part[g, y, b] = total.astype(BF16)
        each(0, n_z, one)
        each(1, n_z, lambda o: t_zr(q, o).start())

    def za_start(q):
        each(1, n_z, lambda o: t_zr(q, o).wait_recv())
        total = part[gid(x, c, q), y, z].astype(F32)
        for o in range(1, n_z):
            total = total + rz[q, o].astype(F32)
        ag[q, y, z] = total.astype(BF16)
        each(1, n_z, lambda o: t_za(q, o).start())

    def ya_start(q):
        each(1, n_z, lambda o: t_za(q, o).wait_recv())
        each(1, n_y, lambda o: t_ya(q, o).start())

    sbuf[...] = jnp.zeros_like(sbuf)

    def backward_group(g, half):
        wl = jnp.where(lower, wmix_ref[g], jnp.zeros((), BF16))
        wlt = wl.T
        bias = bias_ref[g]
        gain = gain_ref[g]
        shift = shift_ref[g]
        acc[...] = jnp.zeros_like(acc)
        wl_ref[...] = wl
        wlt_ref[...] = wlt
        hl = pl.ds(pl.multiple_of(half * chans, chans), chans)
        for b in range(nb):
            at = pl.ds(b * span, span)
            gated, v_slope = gelu_both(v_ref[at, lanes(g)].astype(F32))
            scaled, inverse = norm_parts(gated)
            normed = (scaled * gain + shift).astype(BF16)
            mixed = mm(wl_ref[...], normed, 1, 0) + bias
            upper, u_slope = gelu_both(u_ref[at, lanes(g)].astype(F32))
            cot = gs[at, hl].astype(F32)
            dm = cot * upper
            dmb = dm.astype(BF16)
            gu_ref[at, lanes(g)] = (cot * mixed * u_slope).astype(BF16)
            acc[0] += dm
            acc[1] += mm(dmb, normed, 1, 1)
            dn = mm(wlt_ref[...], dmb, 1, 0)
            acc[2] += dn * scaled
            acc[3] += dn
            e = dn * gain
            m1 = jnp.mean(e, axis=-1, keepdims=True)
            m2 = jnp.mean(e * scaled, axis=-1, keepdims=True)
            gv_ref[at, lanes(g)] = (v_slope * (inverse * (e - m1 - scaled * m2))).astype(BF16)
        grad_w = jnp.where(lower, acc[1], 0.0)
        per = span // part_rows
        for p in range(per):
            sbuf[g * per + p, 0:part_rows, :] = grad_w[p * part_rows : (p + 1) * part_rows].astype(BF16)
        g_bias = jnp.sum(acc[0].T, axis=0, keepdims=True)
        g_gain = jnp.sum(acc[2], axis=0, keepdims=True)
        g_shift = jnp.sum(acc[3], axis=0, keepdims=True)
        r16 = lax.broadcasted_iota(jnp.int32, (16, chans), 0)
        extra = jnp.where(r16 == 0, g_bias, jnp.where(r16 == 1, g_gain, jnp.where(r16 == 2, g_shift, 0.0)))
        sbuf[g * per, part_rows : part_rows + 16, :] = extra.astype(BF16)
        for p in range(per):
            to = g * per + p

            @pl.when(to != me)
            def _(to=to):
                t_s1((to + n_dev - me) % n_dev).start()

    per_chunk = gpc // 2
    flat = wfull.reshape(n_dp, wfull.shape[1] * 2 * wfull.shape[3], wfull.shape[4])

    def stores(i):
        turn = i // per_chunk
        chunk = 2 * down(turn // 2) + (c + turn) % 2
        first = (chunk * gpc + 2 * (i % per_chunk)) * chans
        at = pl.ds(pl.multiple_of(first, 2 * chans), 2 * chans)
        return (
            pltpu.make_async_copy(gu_ref.at[:, at], gu_hbm.at[:, at], gu_s.at[i]),
            pltpu.make_async_copy(gv_ref.at[:, at], gv_hbm.at[:, at], gv_s.at[i]),
        )

    def backward_step(i):
        turn = i // per_chunk
        k = turn // 2
        chunk = 2 * down(k) + (c + turn) % 2
        two = i % per_chunk
        wrows = flat[chunk, pl.ds(pl.multiple_of(two * 2 * span, 2 * span), 2 * span), :]

        def one(j):
            at = pl.ds(pl.multiple_of(j * 2 * span, 2 * span), 2 * span)
            gs[at, :] = mm(d_ref[at, :], wrows, 1, 1).astype(BF16)
        each(0, rows // (2 * span), one)
        each(0, 2, lambda h: backward_group(chunk * gpc + 2 * two + h, h))
        for store in stores(i):
            store.start()

    n_steps = n_dp * per_chunk
    actions = {}

    def put(step, fn):
        actions.setdefault(min(step, n_steps - 1), []).append(fn)

    put(min(2, 2 * per_chunk - 2), forward_w)
    when = ((-1, 1, 3, 5), (0, 2, 4, 6), (2, 4, 6, 8), (4, 6, 8, 9))
    late = []
    stages = (yr_start, zr_start, za_start, ya_start)
    plan = [(when[q % 4][n], n, q) for q in range(gpc) for n in range(4)]
    for step, n, q in sorted(plan):
        fn = functools.partial(stages[n], q)
        if step < 0:
            fn()
        elif step < n_steps:
            put(step, fn)
        else:
            late.append(fn)

    def whole_step(i):
        turn = i // per_chunk
        for k in range(1, pairs):
            @pl.when(i == (2 * k + 1) * per_chunk)
            def _(k=k):
                w_fw(k).wait_recv()
        backward_step(i)
        for step in sorted(actions):
            @pl.when(i == step)
            def _(step=step):
                for fn in actions[step]:
                    fn()

    each(0, n_steps, whole_step)

    for fn in late[:2]:
        fn()
    each(1, n_dev, lambda o: t_s1(o).wait_recv())
    acc_s = sbuf[me].astype(F32)
    acc_s = lax.fori_loop(1, n_dev, lambda o, a: a + srecv[o].astype(F32), acc_s)
    each(1, n_dev, lambda o: t_s1(o).wait_send())
    sbuf[me] = acc_s.astype(BF16)
    srecv[n_dev + me] = acc_s.astype(BF16)
    each(1, n_dev, lambda o: t_s2(o).start())
    for fn in late[2:]:
        fn()

    for q in range(gpc):
        each(1, n_y, lambda o: t_ya(q, o).wait_recv())
        for j in range(n_sp):
            dw_ref[q * span : (q + 1) * span, j * width : (j + 1) * width] = ag[q, j // n_z, j % n_z]

    each(1, n_dev, lambda o: t_s2(o).wait_recv())
    sm_ref[...] = srecv[n_dev : 2 * n_dev]

    def stored(i):
        for store in stores(i):
            store.wait()
    each(0, n_steps, stored)

    w_own().wait_send()
    for k in range(1, pairs):
        w_x(k).wait_send()
        w_z(k).wait_send()
        each(1, n_y, lambda o: w_y(k, 0, o).wait_send())
        each(1, n_y, lambda o: w_y(k, 1, o).wait_send())
        w_fw(k).wait_send()
        each(0, gpc, lambda q: t_x(k, q).wait_send())
    for k in range(pairs):
        each(0, gpc, lambda q: t_core(k, q).wait_send())
    for q in range(gpc):
        each(1, n_y, lambda o: t_yr(q, o).wait_send())
        each(1, n_z, lambda o: t_zr(q, o).wait_send())
        each(1, n_z, lambda o: t_za(q, o).wait_send())
        each(1, n_y, lambda o: t_ya(q, o).wait_send())
    each(1, n_dev, lambda o: t_s2(o).wait_send())


def on_device(n_sp, n_dp, u_pre, v_pre, d_out, w_mix, mix_bias, norm_gain, norm_shift, w_out):
    _, rows, wide = u_pre.shape
    depth = d_out.shape[2]
    groups, span = w_mix.shape[:2]
    chans = wide // groups
    gpc = groups // n_dp
    width = depth // n_sp
    n_dev = n_sp * n_dp
    per = n_dev // groups
    part_rows = span // per
    shard = w_out.shape[0]
    pairs = n_dp // 2
    n_y = 1
    while 4 * n_y * n_y <= n_sp:
        n_y *= 2
    n_z = n_sp // n_y
    dims = (n_y, n_z, n_dp, gpc, span, chans, width, rows)
    dma = pltpu.SemaphoreType.DMA
    vm = pltpu.VMEM
    piece = (n_y, n_z, span, width)
    w_piece = (n_y, 2, shard // (2 * n_y), depth)
    n_steps = groups // 2
    scratch = [
        vm((rows, wide), BF16), vm((rows, wide), BF16), vm((rows, depth), BF16),
        vm((rows, wide), BF16), vm((rows, wide), BF16),
        dma((3,)), dma((n_steps,)), dma((n_steps,)),
        vm((n_dp,) + w_piece, BF16),
        vm((groups,) + piece, BF16),
        vm((pairs, gpc) + piece, BF16),
        vm((pairs, gpc) + piece, BF16),
        vm((gpc,) + piece, BF16),
        vm((gpc,) + piece[1:2] + piece[2:], BF16),
        vm((gpc,) + piece, BF16),
        vm((rows, 2 * chans), BF16),
        vm((2 * chans, rows), BF16),
        vm((span, span), BF16),
        vm((span, span), BF16),
        vm((4, span, chans), F32),
        vm((n_dev, part_rows + 16, chans), BF16),
        vm((2 * n_dev, part_rows + 16, chans), BF16),
        dma, dma,
        dma((pairs,)), dma((pairs,)),
        dma((pairs,)), dma((pairs,)),
        dma((pairs, 2, n_y)), dma((pairs, 2, n_y)),
        dma((pairs,)), dma((pairs,)),
        dma((pairs, gpc)), dma((pairs, gpc)),
        dma((pairs, gpc)), dma((pairs, gpc)),
        dma((gpc, n_y)), dma((gpc, n_y)),
        dma((gpc, n_z)), dma((gpc, n_z)),
        dma((gpc, n_z)), dma((gpc, n_z)),
        dma((gpc, n_y)), dma((gpc, n_y)),
        dma((n_dev,)), dma((n_dev,)),
        dma((n_dev,)), dma((n_dev,)),
    ]
    spec = pl.BlockSpec(memory_space=pltpu.VMEM)
    hbm = pl.BlockSpec(memory_space=pl.ANY)
    gu, gv, dw, sm = pl.pallas_call(
        functools.partial(kernel, dims),
        out_shape=(
            jax.ShapeDtypeStruct((rows, wide), BF16),
            jax.ShapeDtypeStruct((rows, wide), BF16),
            jax.ShapeDtypeStruct((shard, depth), BF16),
            jax.ShapeDtypeStruct((n_dev, part_rows + 16, chans), BF16),
        ),
        in_specs=[hbm] * 3 + [spec] * 5,
        out_specs=(hbm, hbm, spec, spec),
        scratch_shapes=scratch,
        compiler_params=pltpu.CompilerParams(collective_id=0, has_side_effects=True, vmem_limit_bytes=67043328),
    )(
        u_pre[0], v_pre[0], d_out[0], w_mix,
        jnp.broadcast_to(mix_bias[:, :, None], (groups, span, chans)),
        norm_gain[:, None, :], norm_shift[:, None, :],
        w_out.reshape(w_piece),
    )
    grad_w = sm[:, :part_rows].reshape(groups, span, span).astype(F32)
    extra = sm.reshape(groups, per, part_rows + 16, chans)[:, 0, part_rows:].astype(F32)
    return (gu[None], gv[None], dw.astype(F32), grad_w, extra[:, 0], extra[:, 1], extra[:, 2])


def solution(mesh):
    body = functools.partial(on_device, mesh.shape["sp"], mesh.shape["dp"])
    return jax.shard_map(
        body,
        mesh=mesh,
        in_specs=(
            P("dp", "sp", None),
            P("dp", "sp", None),
            P("dp", "sp", None),
            P(),
            P(),
            P(),
            P(),
            P("dp", None),
        ),
        out_specs=(P("dp", "sp", None), P("dp", "sp", None), P("dp", None), P(), P(), P(), P()),
        check_vma=False,
    )
```

profile of v0, /device:TPU:13, one launch (start us, length us, event | category | flops | bytes accessed | tf_op | source)
XLA Modules:
  0.0 157.9 jit_solution(1168826026070746773)
XLA Ops:
  0.6 2.0 %broadcast_in_dim.18.bias_ref = f32[16,128,128]{2,1,0:T(8,128)} broadcast(f32[16,128]{1,0:T(8,128)} %param.12), dimensions={0,1} | broadcast | bytes 1056768 | tf_op jit(solution)/shard_map/broadcast_in_dim | solution.py:501
  2.6 143.5 %shard_map.135 = (bf16[1024,2048]{1,0:T(8,128)(2,1)}, bf16[1024,2048]{1,0:T(8,128)(2,1)}, bf16[512,2048]{1,0:T(8,128)(2,1)}, bf16[32,80,128]{2,1,0:T(8,128)(2,1)}) custom-call(bf16[1024,2048]{1,0:T(8,128)(2,1)} %bitcast.24, bf16[1024,2048]{1,0:T(8,128)(2,1)} %bitcast.25, bf16[1024,2048]{1,0:T(8,128)(2,1)} %bitcast.26, bf16[16,128,128]{2,1,0:T(8,128)(2,1)} %wmix_ref.1, ...), custom_call_target="tpu_custom_call" | custom-call | tf_op jit(solution)/shard_map/pallas_call | solution.py:487
  146.1 0.0 copy-start.2
  146.1 0.0 copy-start.1
  146.1 4.3 %convert_element_type.15 = f32[512,2048]{1,0:T(8,128)} convert(bf16[512,2048]{1,0:T(8,128)(2,1)} %get-tuple-element.13) | non-fusion elementwise | flops 1048576 | bytes 6291456 | tf_op jit(solution)/shard_map/convert_element_type | solution.py:507
  150.4 0.0 copy-done.2
  150.4 0.1 slice.15
  150.5 1.1 bitcast_convert_fusion
  151.6 0.6 slice_bitcast_fusion
  152.2 0.0 copy-done.1
  152.2 0.0 copy-start
  152.2 2.1 %copy.22 = bf16[1,1024,2048]{2,1,0:T(8,128)(2,1)} copy(bf16[1,1024,2048]{2,1,0:T(8,128)(2,1)S(1)} %bitcast.28) | data formatting | bytes 8388608
  154.3 1.6 copy-done
  155.9 2.0 %copy.23 = bf16[1,1024,2048]{2,1,0:T(8,128)(2,1)} copy(bf16[1,1024,2048]{2,1,0:T(8,128)(2,1)S(1)} %bitcast.27) | data formatting | bytes 8388608
  (2 shorter events, 0.0 us)
Async XLA Ops:
  146.1 4.3 %copy-start.2 = (bf16[32,80,128]{2,1,0:T(8,128)(2,1)S(1)}, bf16[32,80,128]{2,1,0:T(8,128)(2,1)}, u32[]{:S(2)}) copy-start(bf16[32,80,128]{2,1,0:T(8,128)(2,1)} %get-tuple-element.14) | copy-start | bytes 1966084
  146.1 6.1 %copy-start.1 = (bf16[1024,2048]{1,0:T(8,128)(2,1)S(1)}, bf16[1024,2048]{1,0:T(8,128)(2,1)}, u32[]{:S(2)}) copy-start(bf16[1024,2048]{1,0:T(8,128)(2,1)} %get-tuple-element.11) | copy-start | bytes 12582916
  152.2 3.7 %copy-start = (bf16[1024,2048]{1,0:T(8,128)(2,1)S(1)}, bf16[1024,2048]{1,0:T(8,128)(2,1)}, u32[]{:S(2)}) copy-start(bf16[1024,2048]{1,0:T(8,128)(2,1)} %get-tuple-element.12) | copy-start | bytes 12582916
where the time goes:
time: 158 us
  Pallas kernels  143 us (91%)
  local copies, waits for them, and re-layouts  8.39 us (5%)
  other arithmetic  5.37 us (3%)
    pallas_call x1, Pallas kernels, on_device(): pl.pallas_call(functools.partial(kernel, dims), out_shape=(jax.ShapeDtype...  143 us
    unnamed x8, local copies, waits for them, and re-layouts  5.72 us
    convert_element_type x1, other arithmetic, on_device(): dw.astype(F32)  4.28 us

commit v1 on v0

v1 whole, which is shorter than its diff:
```python
import functools

import jax
import jax.numpy as jnp
from jax import lax
from jax.experimental import pallas as pl
from jax.experimental.pallas import tpu as pltpu
from jax.sharding import PartitionSpec as P

EPS = 1e-05
K0 = 0.7978845608028654
K1 = 0.044715
F32 = jnp.float32
BF16 = jnp.bfloat16


TIMES = (6.0, 2.4, 27.7, 2.05, 6, 2.5)
T_W = (13.5, 19.5, 21.6, 27.0)
T_WZ = ((0, 2), (3, 5))
T_UNIT = (
    (25.0, 33.5, 39.5, 46.0, 52.0, 58.0, 78.2),
    (37.0, 46.2, 52.0, 58.2, 64.6, 70.0, 78.4),
    (48.0, 56.6, 65.0, 73.0, 81.5),
    (56.5, 62.8, 68.5, 74.0, 81.0),
    (64.0, 69.5, 75.0, 80.5, 86.0),
)
T_END = (65.2, 62.9, 71.5, 69.0, 76.5)


def gelu_parts(a):
    sq = a * a
    t = jnp.tanh(a * (K0 + (K0 * K1) * sq))
    half = 0.5 * (1.0 + t)
    return sq, t, half


def gelu(a):
    _, _, half = gelu_parts(a)
    return a * half


def gelu_both(a):
    sq, t, half = gelu_parts(a)
    slope = half + (0.5 * a) * (1.0 - t * t) * (K0 + (3.0 * K0 * K1) * sq)
    return a * half, slope


def norm_parts(gated):
    centre = gated - jnp.mean(gated, axis=-1, keepdims=True)
    inverse = lax.rsqrt(jnp.mean(centre * centre, axis=-1, keepdims=True) + EPS)
    return centre * inverse, inverse


def mm(a, b, ca, cb):
    return lax.dot_general(a, b, (((ca,), (cb,)), ((), ())), preferred_element_type=F32)


def each(lo, hi, fn):
    def body(i, carry):
        fn(i)
        return carry
    lax.fori_loop(lo, hi, body, 0)


def kernel(
    dims,
    u_hbm, v_hbm, d_hbm, wmix_hbm, bias_hbm, gain_hbm, shift_hbm, w_hbm,
    gu_ref, gv_ref, dw_ref, sm_ref,
    u_ref, v_ref, d_ref, wmix_ref, bias_row, gain_ref, shift_ref, bias_ref, u_s, v_s, in_s,
    wfull, part, rcore, rx, ry, rz, ag, gs, got, wl_ref, wlt_ref, acc,
    sbuf, acore, srecv, fin,
    wown_s, wown_r, wx_s, wx_r, wy_s, wy_r, wz_s, wz_r, wfw_s, wfw_r,
    core_s, core_r, xs_s, xs_r, yr_s, yr_r, zr_s, zr_r, za_s, za_r, ya_s, ya_r,
    sa_s, sa_r, sb_s, sb_r, sc_s, sc_r, sd_s, sd_r,
):
    n_y, n_z, n_dp, gpc, span, chans, width, rows, prow, n_own = dims
    n_sp = n_y * n_z
    pairs = n_dp // 2
    n_chips = n_sp * pairs
    nb = rows // span
    s = lax.axis_index("sp")
    dpi = lax.axis_index("dp")
    x = dpi // 2
    c = dpi % 2
    y = s % n_y
    z = s // n_y
    zp = z % 2
    other = 1 - c
    mate = {"sp": s, "dp": 2 * x + other}
    chip = s * pairs + x

    def rc(src, dst, ssem, rsem, dev):
        return pltpu.make_async_remote_copy(
            src_ref=src, dst_ref=dst, send_sem=ssem, recv_sem=rsem,
            device_id=dev, device_id_type=pl.DeviceIdType.MESH,
        )

    def up(k):
        return (x + k) % pairs

    def down(k):
        return (x + pairs - k) % pairs

    def at_x(k):
        return {"sp": s, "dp": 2 * up(k) + c}

    def at_y(o):
        return {"sp": z * n_y + (y + o) % n_y, "dp": dpi}

    def at_z(o):
        return {"sp": (z + o) % n_z * n_y + y, "dp": dpi}

    def at_chip(o):
        to = (chip + o) % n_chips
        return {"sp": to // pairs, "dp": 2 * (to % pairs) + c}

    def w_own():
        return rc(wfull.at[dpi], wfull.at[dpi], wown_s, wown_r, mate)

    def w_x(k, h):
        block = wfull.at[dpi, y, zp, h]
        return rc(block, block, wx_s.at[k, h], wx_r.at[k, h], at_x(k))

    def w_y(k, h, o):
        block = wfull.at[2 * down(k) + c, y, zp, h]
        return rc(block, block, wy_s.at[k, h, o], wy_r.at[k, h, o], at_y(o))

    def w_z(k, h, o):
        a = (y + o) % n_y
        block = wfull.at[2 * down(k) + c, a, zp, h]
        to = {"sp": (z + 1 - 2 * zp) * n_y + y, "dp": dpi}
        return rc(block, block, wz_s.at[k, h, o], wz_r.at[k, h, o], to)

    def w_fw(k, a, zz, h):
        block = wfull.at[2 * down(k) + c, a, zz, h]
        return rc(block, block, wfw_s.at[k, a, zz, h], wfw_r.at[k, a, zz, h], mate)

    units = [(q, 0, span) for q in range(gpc - 1)]
    units += [(gpc - 1, 0, span // 2), (gpc - 1, span // 2, span // 2)]
    half_z = n_z // 2

    def gid(xx, cc, q):
        return (2 * xx + cc) * gpc + q

    def t_core(k, q):
        return rc(part.at[gid(up(k), other, q)], rcore.at[k, q], core_s.at[k, q], core_r.at[k, q], mate)

    def t_x(k, n, a):
        q, lo, size = units[n]
        at = pl.ds(lo, size)
        return rc(
            part.at[gid(up(k), c, q), a, :, at], rx.at[k - 1, q, a, :, at],
            xs_s.at[k, n, a], xs_r.at[k, n, a], at_x(k),
        )

    def t_yr(n, o, b):
        q, lo, size = units[n]
        at = pl.ds(lo, size)
        return rc(
            part.at[gid(x, c, q), (y + o) % n_y, b, at], ry.at[q, o - 1, b, at],
            yr_s.at[n, o], yr_r.at[n, o, b], at_y(o),
        )

    def all_yr(n, o):
        q, lo, size = units[n]
        block = part.at[gid(x, c, q), (y + o) % n_y, :, pl.ds(lo, size)]
        return rc(block, block, yr_s.at[n, o], yr_r.at[n, o, 0], mate)

    def z_send(n, b, slot, dst_slot, to):
        q, lo, size = units[n]
        at = pl.ds(lo, size)
        return rc(
            part.at[gid(x, c, q), y, b, at], rz.at[q, dst_slot, at],
            zr_s.at[n, slot], zr_r.at[n, slot], to,
        )

    to_pair = {"sp": (z + 1 - 2 * zp) * n_y + y, "dp": dpi}
    pair_z = z + 1 - 2 * zp

    def t_zr(n, o):
        return z_send(n, (z + o) % n_z, o, o - 1, at_z(o))

    def t_zp(n, m):
        return z_send(n, (pair_z + 2 * m) % n_z, 2 * m + 1, m, to_pair)

    def t_zc(n, m):
        return z_send(n, (z + 2 * m) % n_z, 2 * m, half_z + m - 1, at_z(2 * m))

    def gathered(n, b, ssem, rsem, to):
        q, lo, size = units[n]
        block = ag.at[q, y, b, pl.ds(lo, size)]
        return rc(block, block, ssem, rsem, to)

    def t_za(n, o):
        return gathered(n, z, za_s.at[n, o], za_r.at[n, o], at_z(o))

    def t_ap(n, m):
        return gathered(n, (z + 2 * m) % n_z, za_s.at[n, 2 * m + 1], za_r.at[n, 2 * m + 1], to_pair)

    def t_ya(n, o, b):
        return gathered(n, b, ya_s.at[n, o], ya_r.at[n, o], at_y(o))

    def all_ya(n, o):
        q, lo, size = units[n]
        block = ag.at[q, y, :, pl.ds(lo, size)]
        return rc(block, block, ya_s.at[n, o], ya_r.at[n, o], mate)

    def t_sa(k, j):
        chunk = 2 * down(k) + j
        return rc(sbuf.at[chunk, other], acore.at[chunk], sa_s.at[chunk], sa_r.at[chunk], mate)

    def t_sb(chunk, o):
        to = (chip + o) % n_chips
        return rc(sbuf.at[chunk, c, to % n_own], srecv.at[chunk, o - 1], sb_s.at[chunk], sb_r.at[chunk], at_chip(o))

    def t_sc(j, o):
        block = fin.at[j, c, chip % n_own]
        return rc(block, block, sc_s.at[j], sc_r.at[j], at_chip(o))

    def all_sb(chunk):
        return rc(srecv.at[chunk], srecv.at[chunk], sb_s.at[chunk], sb_r.at[chunk], mate)

    def all_sc(j):
        block = fin.at[j, c, pl.ds(0, n_own - 1)]
        return rc(block, block, sc_s.at[j], sc_r.at[j], mate)

    def t_sd(j):
        return rc(fin.at[j, c], fin.at[j, c], sd_s.at[j], sd_r.at[j], mate)

    def owner(t, fn):
        if n_own == n_chips:
            fn()
        else:
            pl.when(t < n_own)(fn)

    row = lax.broadcasted_iota(jnp.int32, (span, span), 0)
    col = lax.broadcasted_iota(jnp.int32, (span, span), 1)
    lower = row >= col
    share = 2 * gpc * chans

    def cols(k):
        return pl.ds(pl.multiple_of(up(k) * share, share), share)

    small = [
        pltpu.make_async_copy(src, dst, in_s.at[n])
        for n, (src, dst) in enumerate((
            (bias_hbm, bias_row), (gain_hbm, gain_ref), (shift_hbm, shift_ref), (wmix_hbm, wmix_ref),
        ))
    ]
    near = {k: (
        pltpu.make_async_copy(v_hbm.at[:, cols(k)], v_ref.at[:, cols(k)], v_s.at[k]),
        pltpu.make_async_copy(u_hbm.at[:, cols(k)], u_ref.at[:, cols(k)], u_s.at[k]),
    ) for k in range(pairs)}
    first_k = 1 % pairs
    load_w = pltpu.make_async_copy(w_hbm, wfull.at[dpi], in_s.at[4])
    load_d = pltpu.make_async_copy(d_hbm, d_ref, in_s.at[5])
    for load in small:
        load.start()
    for load in near[first_k]:
        load.start()
    load_w.start()
    load_d.start()
    for k in range(pairs):
        if k != first_k:
            for load in near[k]:
                load.start()
    barrier = pltpu.get_barrier_semaphore()
    pl.semaphore_signal(barrier, inc=1, device_id=mate, device_id_type=pl.DeviceIdType.MESH)
    each(1, n_chips, lambda o: pl.semaphore_signal(
        barrier, inc=1, device_id=at_chip(o), device_id_type=pl.DeviceIdType.MESH,
    ))

    def lanes(g):
        return pl.ds(pl.multiple_of(g * chans, chans), chans)

    def far_group(i, h):
        return gid(up((i // gpc + 1) % pairs), (c + h) % 2, i % gpc)

    def low_weights(g, h):
        wl_ref[h] = jnp.where(lower, wmix_ref[g], jnp.zeros((), BF16))

    def forward_block(i, b):
        at = pl.ds(pl.multiple_of(b * span, span), span)
        for h in range(2):
            g = far_group(i, h)
            scaled, _ = norm_parts(gelu(v_ref[at, lanes(g)].astype(F32)))
            normed = (scaled * gain_ref[g] + shift_ref[g]).astype(BF16)
            mixed = mm(wl_ref[h], normed, 1, 0) + bias_ref[g]
            out = (gelu(u_ref[at, lanes(g)].astype(F32)) * mixed).astype(BF16)
            got[i % 2, h * span : (h + 1) * span, at] = out.T

    def core_sum(k, q):
        t_core(k, q).wait_recv()
        g = gid(up(k), c, q)

        def one(j):
            a, b = j // n_z, j % n_z
            part[g, a, b] = (part[g, a, b].astype(F32) + rcore[k, q, a, b].astype(F32)).astype(BF16)
        each(0, n_sp, one)

    def x_start(k, n):
        for o in range(n_y):
            t_x(k, n, (y + 1 + o) % n_y).start()

    per_block = n_sp // nb

    def product_block(i, b):
        keep = far_group(i, 0)
        give = far_group(i, 1)
        wide = per_block * width
        r = mm(got[i % 2], d_ref[:, pl.ds(pl.multiple_of(b * wide, wide), wide)], 1, 0)
        for e in range(per_block):
            j = b * per_block + e
            at = slice(e * width, (e + 1) * width)
            part[keep, j // n_z, j % n_z] = r[:span, at].astype(BF16)
            part[give, j // n_z, j % n_z] = r[span:, at].astype(BF16)

    def give_core(i):
        t_core((i // gpc + 1) % pairs, i % gpc).start()

    def w_from_x(h):
        for k in range(1, pairs):
            w_x(k, h).wait_recv()
            for o in range(1, n_y):
                w_y(k, h, o).start()
            w_z(k, h, 0).start()
            w_fw(k, y, zp, h).start()

    def w_from_y(h):
        for k in range(1, pairs):
            for o in range(1, n_y):
                w_y(k, h, o).wait_recv()
            for o in range(1, n_y):
                w_z(k, h, o).start()
                w_fw(k, (y + o) % n_y, zp, h).start()

    def w_from_z(h, o):
        for k in range(1, pairs):
            w_z(k, h, o).wait_recv()
            w_fw(k, (y + o) % n_y, 1 - zp, h).start()

    def w_ready(k):
        for h in range(2):
            for zz in range(2):
                for a in range(n_y):
                    w_fw(k, a, zz, h).wait_recv()

    def yr_start(n):
        q, lo, size = units[n]
        if lo == 0:
            t_core(0, q).wait_recv()
        at = pl.ds(lo, size)
        g = gid(x, c, q)
        for o in range(1, n_y):
            a = (y + o) % n_y
            for k in range(1, pairs):
                t_x(k, n, a).wait_recv()

            def one(b):
                total = part[g, a, b, at].astype(F32) + rcore[0, q, a, b, at].astype(F32)
                for k in range(1, pairs):
                    total = total + rx[k - 1, q, a, b, at].astype(F32)
                part[g, a, b, at] = total.astype(BF16)
                t_yr(n, o, b).start()
            each(1, n_z + 1, lambda j: one((z + j) % n_z))

    def own_total(n, b):
        q, lo, size = units[n]
        at = pl.ds(lo, size)
        total = part[gid(x, c, q), y, b, at].astype(F32) + rcore[0, q, y, b, at].astype(F32)
        for k in range(1, pairs):
            total = total + rx[k - 1, q, y, b, at].astype(F32)
        for o in range(1, n_y):
            total = total + ry[q, o - 1, b, at].astype(F32)
        return total

    def own_ready(n):
        for k in range(1, pairs):
            t_x(k, n, y).wait_recv()

    def y_ready(n, b):
        for o in range(1, n_y):
            t_yr(n, o, b).wait_recv()

    def keep_sum(n, b, total):
        q, lo, size = units[n]
        part[gid(x, c, q), y, b, pl.ds(lo, size)] = total.astype(BF16)

    def from_z(n, slot):
        q, lo, size = units[n]
        return rz[q, slot, pl.ds(lo, size)].astype(F32)

    def whole(n, total):
        q, lo, size = units[n]
        ag[q, y, z, pl.ds(lo, size)] = total.astype(BF16)
        for o in range(1, n_y):
            t_ya(n, o, z).start()

    def zr_start(n):
        own_ready(n)
        for j in range(1, n_z):
            b = (z + j) % n_z
            y_ready(n, b)
            keep_sum(n, b, own_total(n, b))
            t_zr(n, j).start()

    def za_start(n):
        y_ready(n, z)
        total = own_total(n, z)
        for o in range(1, n_z):
            t_zr(n, o).wait_recv()
            total = total + from_z(n, o - 1)
        whole(n, total)
        for o in range(1, n_z):
            t_za(n, o).start()

    def ya_start(n):
        for o in range(1, n_z):
            t_za(n, o).wait_recv()
            for a in range(1, n_y):
                t_ya(n, a, (z + n_z - o) % n_z).start()

    def zp_start(n):
        own_ready(n)
        for j in range(half_z):
            m = half_z - 1 - j
            b = (pair_z + 2 * m) % n_z
            y_ready(n, b)
            keep_sum(n, b, own_total(n, b))
            t_zp(n, m).start()

    def zc_start(n):
        for m in range(1, half_z):
            b = (z + 2 * m) % n_z
            y_ready(n, b)
            t_zp(n, m).wait_recv()
            keep_sum(n, b, own_total(n, b) + from_z(n, m))
            t_zc(n, m).start()

    def ac_start(n):
        y_ready(n, z)
        t_zp(n, 0).wait_recv()
        total = own_total(n, z) + from_z(n, 0)
        for m in range(1, half_z):
            t_zc(n, m).wait_recv()
            total = total + from_z(n, half_z + m - 1)
        whole(n, total)
        for m in range(1, half_z):
            t_za(n, 2 * m).start()
        t_ap(n, 0).start()

    def ap_start(n):
        for m in range(1, half_z):
            t_za(n, 2 * m).wait_recv()
            t_ap(n, half_z - m).start()
            for a in range(1, n_y):
                t_ya(n, a, (z + n_z - 2 * m) % n_z).start()

    def yb_start(n):
        for m in range(half_z):
            t_ap(n, m).wait_recv()
            for a in range(1, n_y):
                t_ya(n, a, (pair_z + 2 * m) % n_z).start()

    def dw_done(n):
        q, lo, size = units[n]
        for o in range(1, n_y):
            all_ya(n, o).wait_recv()

        def one(j):
            dw_ref[q, j, pl.ds(lo, size)] = ag[q, j // n_z, j % n_z, pl.ds(lo, size)]
        each(0, n_sp, one)

    def bias_column(g):
        bias_ref[g] = jnp.broadcast_to(bias_row[g], (span, span)).T

    for load in small:
        load.wait()
    each(0, n_dp * gpc, lambda g: bias_column(g))
    for load in near[first_k]:
        load.wait()
    for h in range(2):
        low_weights(far_group(0, h), h)

    def first_blocks(b):
        for n in range(4):
            forward_block(0, 4 * b + n)
    each(0, nb // 4, first_blocks)
    load_w.wait()
    pl.semaphore_wait(barrier, n_chips)
    for h in range(2):
        for k in range(1, pairs):
            w_x(k, h).start()
    w_own().start()
    load_d.wait()
    for k in range(pairs):
        if k != first_k:
            for load in near[k]:
                load.wait()

    n_far = (pairs - 1) * gpc
    n_fwd = pairs * gpc
    per_chunk = gpc // 2
    n_steps = n_dp * per_chunk
    n_slots = 2 * n_steps
    before = {}
    after = {}
    late = []

    def run(todo):
        for fn, args in todo:
            fn(*args)

    def sa_start(k, j):
        t_sa(k, j).start()

    def sb_start(k, j):
        t_sa(k, j).wait_recv()
        chunk = 2 * down(k) + j

        def one(p):
            sbuf[chunk, c, p] = (sbuf[chunk, c, p].astype(F32) + acore[chunk, p].astype(F32)).astype(BF16)
        each(0, n_own, one)
        each(1, n_chips, lambda o: owner((chip + o) % n_chips, lambda: t_sb(chunk, o).start()))

    def sc_start(j):
        def mine():
            for xx in range(pairs):
                chunk = 2 * xx + j
                all_sb(chunk).wait_recv()
                total = lax.fori_loop(
                    1, n_chips, lambda o, a: a + srecv[chunk, o - 1].astype(F32),
                    sbuf[chunk, c, chip % n_own].astype(F32),
                )
                fin[j, c, chip % n_own, xx] = total.astype(BF16)
            each(1, n_chips, lambda o: t_sc(j, o).start())
        owner(chip, mine)

    def sd_start(j):
        if n_own == n_chips:
            all_sc(j).wait_recv()
        else:
            each(1, n_chips, lambda o: owner((chip + n_chips - o) % n_chips, lambda: t_sc(j, o).wait_recv()))
        t_sd(j).start()

    fwd_0, fwd_us, bwd_0, bwd_us, pause_at, pause_us = TIMES

    def put(time, fn, *args):
        step = 0
        while step <= n_fwd and fwd_0 + fwd_us * step < time:
            step += 1
        at_slot = 0
        while at_slot < n_slots and bwd_0 + bwd_us * (at_slot + 1) + pause_us * (at_slot >= pause_at) < time:
            at_slot += 1
        if step <= n_fwd:
            before.setdefault(max(step, 1), []).append((time, fn, args))
        elif at_slot < n_slots:
            after.setdefault(at_slot, []).append((time, fn, args))
        else:
            late.append((time, fn, args))

    def put_slot(at_slot, time, fn, *args):
        if at_slot < n_slots:
            after.setdefault(at_slot, []).append((time, fn, args))
        else:
            late.append((time, fn, args))

    def in_order(todo):
        return [(fn, args) for _, fn, args in sorted(todo, key=lambda item: item[0])]

    put(T_W[0], w_from_x, 0)
    put(T_W[1], w_from_x, 1)
    put(T_W[2], w_from_y, 0)
    put(T_W[3], w_from_y, 1)
    need = 4 * per_chunk - 3
    for h in range(2):
        for o in range(n_y):
            put_slot(min(need, T_WZ[min(o, 1)][h]), 0.0 + o + h / 2, w_from_z, h, o)
    pair_stages = (yr_start, zp_start, zc_start, ac_start, ap_start, yb_start, dw_done)
    line_stages = (yr_start, zr_start, za_start, ya_start, dw_done)
    for n in range(len(units)):
        when = T_UNIT[n + 5 - len(units)]
        stages = line_stages if len(when) == 5 else pair_stages
        for fn, time in zip(stages, when):
            put(time, fn, n)
    for turn in range(n_dp):
        end = 2 * (turn + 1) * per_chunk
        put_slot(end - 1, 0.0, sa_start, turn // 2, turn % 2)
        put_slot(end, 0.5 if end < n_slots else T_END[0], sb_start, turn // 2, turn % 2)
    put(T_END[1], sc_start, 0)
    put(T_END[2], sc_start, 1)
    put(T_END[3], sd_start, 0)
    put(T_END[4], sd_start, 1)

    def sd_done():
        for j in range(2):
            t_sd(j).wait_recv()
    put(1000.0, sd_done)

    def core_sums(last):
        @pl.when((last >= 0) & (last < n_far))
        def _():
            k = (last // gpc + 1) % pairs
            core_sum(k, last % gpc)
            for kk in range(1, pairs):
                for n, unit in enumerate(units):
                    @pl.when(last == (kk - 1) * gpc + unit[0])
                    def _(kk=kk, n=n):
                        x_start(kk, n)

    def forward_step(i):
        for h in range(2):
            low_weights(far_group(i, h), h)

        def one(b):
            for n in range(4):
                product_block(i - 1, 4 * b + n)
            for n in range(4):
                forward_block(i, 4 * b + n)
        each(0, nb // 4, one)
        give_core(i - 1)
        core_sums(i - 2)
        for step in sorted(before):
            @pl.when(i == step)
            def _(step=step):
                run(in_order(before[step]))

    each(1, n_fwd, forward_step)
    each(0, nb, lambda b: product_block(n_fwd - 1, b))
    give_core(n_fwd - 1)
    core_sums(n_fwd - 2)
    core_sums(n_fwd - 1)
    w_own().wait_recv()
    run(in_order(before.get(n_fwd, [])))

    def backward_block(i, p):
        chunk, two = place(i)
        first = chunk * gpc + 2 * two
        for h in range(2):
            g = first + h
            gain = gain_ref[g]
            for e in range(2):
                at = pl.ds(pl.multiple_of((2 * p + e) * span, span), span)
                gated, v_slope = gelu_both(v_ref[at, lanes(g)].astype(F32))
                scaled, inverse = norm_parts(gated)
                normed = (scaled * gain + shift_ref[g]).astype(BF16)
                mixed = mm(wl_ref[h], normed, 1, 0) + bias_ref[g]
                upper, u_slope = gelu_both(u_ref[at, lanes(g)].astype(F32))
                cot = gs[i % 2, at, h * chans : (h + 1) * chans].astype(F32)
                dm = cot * upper
                dmb = dm.astype(BF16)
                gu_ref[at, lanes(g)] = (cot * mixed * u_slope).astype(BF16)
                acc[h, 0] += dm
                acc[h, 1] += mm(dmb, normed, 1, 1)
                dn = mm(wlt_ref[h], dmb, 1, 0)
                acc[h, 2] += dn * scaled
                acc[h, 3] += dn
                e_ = dn * gain
                m1 = jnp.mean(e_, axis=-1, keepdims=True)
                m2 = jnp.mean(e_ * scaled, axis=-1, keepdims=True)
                gv_ref[at, lanes(g)] = (v_slope * (inverse * (e_ - m1 - scaled * m2))).astype(BF16)

    def group_sums(h, chunk, q):
        grad_w = jnp.where(lower, acc[h, 1], 0.0)
        g_bias = jnp.sum(acc[h, 0].T, axis=0, keepdims=True)
        g_gain = jnp.sum(acc[h, 2], axis=0, keepdims=True)
        g_shift = jnp.sum(acc[h, 3], axis=0, keepdims=True)
        r16 = lax.broadcasted_iota(jnp.int32, (16, chans), 0)
        c16 = lax.broadcasted_iota(jnp.int32, (16, chans), 1)
        extra = jnp.where(r16 % 3 == 0, g_bias, jnp.where(r16 % 3 == 1, g_gain, g_shift))
        turned = pltpu.roll(extra, chans // 2, 1)
        top = jnp.where(c16 < chans // 2, grad_w[:16], jnp.where(r16 < 3, turned, jnp.where(r16 < 6, extra, 0.0)))
        per = span // prow
        hq = gpc // 2
        first = q % hq * per
        for p in range(per):
            block = grad_w[p * prow : (p + 1) * prow]
            if p == 0:
                block = jnp.concatenate([top, block[16:]], axis=0) if prow > 16 else top
            sbuf[chunk, q // hq, first + p] = block.astype(BF16)

    flat = wfull.reshape(n_dp, wfull.shape[1] * wfull.shape[2] * wfull.shape[3] * wfull.shape[4], wfull.shape[5])

    def place(i):
        turn = i // per_chunk
        return 2 * down(turn // 2) + turn % 2, i % per_chunk

    def cotangent_block(i, p):
        chunk, two = place(i)
        at = pl.ds(pl.multiple_of(p * 2 * span, 2 * span), 2 * span)
        these = pl.ds(pl.multiple_of(two * 2 * span, 2 * span), 2 * span)
        gs[i % 2, at, :] = mm(d_ref[at, :], flat[chunk, these, :], 1, 1).astype(BF16)

    n_pairs = nb // 2
    each(0, n_pairs, lambda p: cotangent_block(0, p))

    def slot(t):
        i = t // 2
        chunk, two = place(i)

        @pl.when(t % 2 == 0)
        def _():
            for k in range(1, pairs):
                @pl.when(i + 1 == 2 * k * per_chunk)
                def _(k=k):
                    w_ready(k)
            acc[...] = jnp.zeros_like(acc)
            for h in range(2):
                low_weights(chunk * gpc + 2 * two + h, h)
                wlt_ref[h] = wl_ref[h].T

        def one(p):
            for u in range(2):
                cotangent_block((i + 1) % n_steps, 2 * p + u)
            for u in range(2):
                backward_block(i, 2 * p + u)
        each(t % 2 * (n_pairs // 4), (t % 2 + 1) * (n_pairs // 4), one)

        @pl.when(t % 2 == 1)
        def _():
            for h in range(2):
                group_sums(h, chunk, 2 * two + h)
        for step in sorted(after):
            @pl.when(t == step)
            def _(step=step):
                run(in_order(after[step]))

    each(0, n_slots, slot)
    run(in_order(late))
    sm_ref[...] = fin[...]

    w_own().wait_send()
    for k in range(1, pairs):
        for h in range(2):
            w_x(k, h).wait_send()
            for o in range(n_y):
                w_z(k, h, o).wait_send()
            for o in range(1, n_y):
                w_y(k, h, o).wait_send()
        for h in range(2):
            for zz in range(2):
                each(0, n_y, lambda a: w_fw(k, a, zz, h).wait_send())
        for n in range(len(units)):
            each(0, n_y, lambda a: t_x(k, n, a).wait_send())
    for k in range(pairs):
        each(0, gpc, lambda q: t_core(k, q).wait_send())

    for n in range(len(units)):
        for o in range(1, n_y):
            all_yr(n, o).wait_send()
            all_ya(n, o).wait_send()
        if len(T_UNIT[n + 5 - len(units)]) == 5:
            for o in range(1, n_z):
                t_zr(n, o).wait_send()
                t_za(n, o).wait_send()
        else:
            for m in range(half_z):
                t_zp(n, m).wait_send()
                t_ap(n, m).wait_send()
            for m in range(1, half_z):
                t_zc(n, m).wait_send()
                t_za(n, 2 * m).wait_send()
    for k in range(pairs):
        for j in range(2):
            t_sa(k, j).wait_send()
    if n_own == n_chips:
        each(0, n_dp, lambda chunk: all_sb(chunk).wait_send())
    else:
        each(0, n_dp, lambda chunk: each(1, n_chips, lambda o: owner((chip + o) % n_chips, lambda: t_sb(chunk, o).wait_send())))
    for j in range(2):
        if n_own == n_chips:
            all_sc(j).wait_send()
        else:
            owner(chip, lambda: each(1, n_chips, lambda o: t_sc(j, o).wait_send()))
        t_sd(j).wait_send()


def finish(dims, gu_ref, gv_ref, dw_ref, sm_ref, gu_hbm, gv_hbm, dw_hbm, gw_hbm, bias_ref, gain_ref, shift_ref, dw_f, gw_f, sem, dw_sem):
    gpc, span, chans, width, n_sp, groups, prow = dims
    copies = [
        pltpu.make_async_copy(gu_ref, gu_hbm.at[0], sem.at[0]),
        pltpu.make_async_copy(gv_ref, gv_hbm.at[0], sem.at[1]),
    ]
    for copy in copies:
        copy.start()
    for q in range(gpc):
        for j in range(n_sp):
            dw_f[q * span : (q + 1) * span, j * width : (j + 1) * width] = dw_ref[q, j].astype(F32)
        at = pl.ds(q * span, span)
        copy = pltpu.make_async_copy(dw_f.at[at], dw_hbm.at[at], dw_sem.at[q])
        copy.start()
        copies.append(copy)
    r = lax.broadcasted_iota(jnp.int32, (prow, chans), 0)
    l = lax.broadcasted_iota(jnp.int32, (prow, chans), 1)
    per = span // prow
    hq = gpc // 2
    for g in range(groups):
        chunk, q = divmod(g, gpc)
        xx, j = divmod(chunk, 2)
        for p in range(per):
            block = sm_ref[j, q // hq, q % hq * per + p, xx].astype(F32)
            gw_f[g, p * prow : (p + 1) * prow, :] = jnp.where(r + p * prow >= l, block, 0.0)
            if p == 0:
                turned = pltpu.roll(block[:8], chans // 2, 1)
                for n, ref in enumerate((bias_ref, gain_ref, shift_ref)):
                    ref[g : g + 1, :] = jnp.where(l[:1] < chans // 2, turned[n : n + 1], block[n + 3 : n + 4])
    copy = pltpu.make_async_copy(gw_f, gw_hbm, sem.at[2])
    copy.start()
    copies.append(copy)
    for copy in copies:
        copy.wait()


def on_device(n_sp, n_dp, u_pre, v_pre, d_out, w_mix, mix_bias, norm_gain, norm_shift, w_out):
    _, rows, wide = u_pre.shape
    depth = d_out.shape[2]
    groups, span = w_mix.shape[:2]
    chans = wide // groups
    gpc = groups // n_dp
    width = depth // n_sp
    shard = w_out.shape[0]
    pairs = n_dp // 2
    n_chips = n_sp * pairs
    half_rows = gpc // 2 * span
    prow = max(16, half_rows // n_chips)
    n_own = half_rows // prow
    n_y = 1
    while 4 * n_y * n_y <= n_sp:
        n_y *= 2
    n_z = n_sp // n_y
    dims = (n_y, n_z, n_dp, gpc, span, chans, width, rows, prow, n_own)
    dma = pltpu.SemaphoreType.DMA
    vm = pltpu.VMEM
    piece = (n_y, n_z, span, width)
    w_piece = (n_y, 2, 2, shard // (4 * n_y), depth)
    scratch = [
        vm((rows, wide), BF16), vm((rows, wide), BF16), vm((rows, depth), BF16),
        vm((groups, span, span), BF16),
        vm((groups, 1, span), F32), vm((groups, 1, chans), F32), vm((groups, 1, chans), F32),
        vm((groups, span, chans), F32),
        dma((pairs,)), dma((pairs,)), dma((6,)),
        vm((n_dp,) + w_piece, BF16),
        vm((groups,) + piece, BF16),
        vm((pairs, gpc) + piece, BF16),
        vm((pairs - 1, gpc) + piece, BF16),
        vm((gpc, n_y - 1) + piece[1:], BF16),
        vm((gpc, n_z - 1) + piece[2:], BF16),
        vm((gpc,) + piece, BF16),
        vm((2, rows, 2 * chans), BF16),
        vm((2, 2 * chans, rows), BF16),
        vm((2, span, span), BF16),
        vm((2, span, span), BF16),
        vm((2, 4, span, chans), F32),
        vm((n_dp, 2, n_own, prow, chans), BF16),
        vm((n_dp, n_own, prow, chans), BF16),
        vm((n_dp, n_chips - 1, prow, chans), BF16),
        vm((2, 2, n_own, pairs, prow, chans), BF16),
        dma, dma,
        dma((pairs, 2)), dma((pairs, 2)),
        dma((pairs, 2, n_y)), dma((pairs, 2, n_y)),
        dma((pairs, 2, n_y)), dma((pairs, 2, n_y)),
        dma((pairs, n_y, 2, 2)), dma((pairs, n_y, 2, 2)),
        dma((pairs, gpc)), dma((pairs, gpc)),
        dma((pairs, gpc + 1, n_y)), dma((pairs, gpc + 1, n_y)),
        dma((gpc + 1, n_y)), dma((gpc + 1, n_y, n_z)),
        dma((gpc + 1, n_z)), dma((gpc + 1, n_z)),
        dma((gpc + 1, n_z)), dma((gpc + 1, n_z)),
        dma((gpc + 1, n_y)), dma((gpc + 1, n_y)),
        dma((n_dp,)), dma((n_dp,)),
        dma((n_dp,)), dma((n_dp,)),
        dma((2,)), dma((2,)),
        dma((2,)), dma((2,)),
    ]
    spec = pl.BlockSpec(memory_space=pltpu.VMEM)
    hbm = pl.BlockSpec(memory_space=pl.ANY)
    results = pl.pallas_call(
        functools.partial(kernel, dims),
        out_shape=(
            vm((rows, wide), BF16),
            vm((rows, wide), BF16),
            vm((gpc, n_sp, span, width), BF16),
            vm((2, 2, n_own, pairs, prow, chans), BF16),
        ),
        in_specs=[hbm] * 8,
        out_specs=(spec,) * 4,
        scratch_shapes=scratch,
        compiler_params=pltpu.CompilerParams(
            collective_id=0, has_side_effects=True, vmem_limit_bytes=48 * 1024 * 1024,
        ),
    )(
        u_pre[0], v_pre[0], d_out[0], w_mix,
        mix_bias[:, None, :], norm_gain[:, None, :], norm_shift[:, None, :],
        w_out.reshape(w_piece),
    )
    return pl.pallas_call(
        functools.partial(finish, (gpc, span, chans, width, n_sp, groups, prow)),
        out_shape=(
            jax.ShapeDtypeStruct((1, rows, wide), BF16),
            jax.ShapeDtypeStruct((1, rows, wide), BF16),
            jax.ShapeDtypeStruct((shard, depth), F32),
            jax.ShapeDtypeStruct((groups, span, span), F32),
            jax.ShapeDtypeStruct((groups, span), F32),
            jax.ShapeDtypeStruct((groups, chans), F32),
            jax.ShapeDtypeStruct((groups, chans), F32),
        ),
        in_specs=[spec] * 4,
        out_specs=(hbm,) * 4 + (spec,) * 3,
        scratch_shapes=[
            vm((shard, depth), F32), vm((groups, span, span), F32), dma((3,)), dma((gpc,)),
        ],
        compiler_params=pltpu.CompilerParams(vmem_limit_bytes=32 * 1024 * 1024),
    )(*[pltpu.with_memory_space_constraint(r, pltpu.VMEM) for r in results])


def solution(mesh):
    body = functools.partial(on_device, mesh.shape["sp"], mesh.shape["dp"])
    return jax.shard_map(
        body,
        mesh=mesh,
        in_specs=(
            P("dp", "sp", None),
            P("dp", "sp", None),
            P("dp", "sp", None),
            P(),
            P(),
            P(),
            P(),
            P("dp", None),
        ),
        out_specs=(P("dp", "sp", None), P("dp", "sp", None), P("dp", None), P(), P(), P(), P()),
        check_vma=False,
    )
```

time: 158 us -> 110 us (0.70)
  the two profiles are of different devices: /device:TPU:13 before, /device:TPU:0 now
where the time goes in v1:
time: 110 us
  Pallas kernels  109 us (99%)
    pallas_call x1, Pallas kernels, on_device(): pl.pallas_call(functools.partial(kernel, dims), out_shape=(vm((rows, wide...  104 us
    pallas_call x1, Pallas kernels, on_device(): pl.pallas_call(functools.partial(finish, (gpc, span, chans, width, n_sp,...  5.55 us

profile of v1, /device:TPU:0, one launch (start us, length us, event | category | flops | bytes accessed | tf_op | source)
XLA Modules:
  0.0 109.7 jit_solution(18122142912734446313)
XLA Ops:
  0.6 103.5 %shard_map.135 = (bf16[1024,2048]{1,0:T(8,128)(2,1)S(1)}, bf16[1024,2048]{1,0:T(8,128)(2,1)S(1)}, bf16[4,8,128,256]{3,2,1,0:T(8,128)(2,1)S(1)}, bf16[2,2,16,2,16,128]{5,4,3,2,1,0:T(8,128)(2,1)S(1)}) custom-call(bf16[1024,2048]{1,0:T(8,128)(2,1)} %bitcast.7, bf16[1024,2048]{1,0:T(8,128)(2,1)} %bitcast.8, bf16[1024,2048]{1,0:T(8,128)(2,1)} %bitcast.9, ...), custom_call_target="tpu_custom_call" | custom-call | tf_op jit(solution)/shard_map/pallas_call | solution.py:876
  104.2 5.5 %shard_map.136 = (bf16[1,1024,2048]{2,1,0:T(8,128)(2,1)}, bf16[1,1024,2048]{2,1,0:T(8,128)(2,1)}, f32[512,2048]{1,0:T(8,128)}, f32[16,128,128]{2,1,0:T(8,128)}, ...) custom-call(bf16[1024,2048]{1,0:T(8,128)(2,1)S(1)} %get-tuple-element.11.gu_ref, ...), custom_call_target="tpu_custom_call" | custom-call | tf_op jit(solution)/shard_map/pallas_call | solution.py:895

commit v2 on v1

--- a/solution.py
+++ b/solution.py
@@ -18,13 +18,13 @@
 T_W = (13.5, 19.5, 21.6, 27.0)
 T_WZ = ((0, 2), (3, 5))
 T_UNIT = (
-    (25.0, 33.5, 39.5, 46.0, 52.0, 58.0, 78.2),
-    (37.0, 46.2, 52.0, 58.2, 64.6, 70.0, 78.4),
-    (48.0, 56.6, 65.0, 73.0, 81.5),
-    (56.5, 62.8, 68.5, 74.0, 81.0),
-    (64.0, 69.5, 75.0, 80.5, 86.0),
+    (25.0, 33.5, 43.0, 50.5, 56.8, 64.9, 80.7),
+    (37.0, 46.2, 52.0, 58.2, 64.85, 69.5, 80.8),
+    (48.0, 56.6, 64.4, 72.0, 84.0),
+    (56.5, 62.8, 69.0, 75.0, 83.0),
+    (64.0, 69.3, 75.2, 80.4, 86.0),
 )
-T_END = (65.2, 62.9, 71.5, 69.0, 76.5)
+T_END = (64.6, 64.8, 70.0, 76.0, 81.0, 69.7, 75.5, 80.5, 85.5)
 
 
 def gelu_parts(a):
@@ -68,10 +68,10 @@
     gu_ref, gv_ref, dw_ref, sm_ref,
     u_ref, v_ref, d_ref, wmix_ref, bias_row, gain_ref, shift_ref, bias_ref, u_s, v_s, in_s,
     wfull, part, rcore, rx, ry, rz, ag, gs, got, wl_ref, wlt_ref, acc,
-    sbuf, acore, srecv, fin,
+    sbuf, acore, s1r, s2r, fin,
     wown_s, wown_r, wx_s, wx_r, wy_s, wy_r, wz_s, wz_r, wfw_s, wfw_r,
     core_s, core_r, xs_s, xs_r, yr_s, yr_r, zr_s, zr_r, za_s, za_r, ya_s, ya_r,
-    sa_s, sa_r, sb_s, sb_r, sc_s, sc_r, sd_s, sd_r,
+    sa_s, sa_r, s1_s, s1_r, s2_s, s2_r, s3_s, s3_r, s4_s, s4_r, sd_s, sd_r,
 ):
     n_y, n_z, n_dp, gpc, span, chans, width, rows, prow, n_own = dims
     n_sp = n_y * n_z
@@ -87,7 +87,11 @@
     zp = z % 2
     other = 1 - c
     mate = {"sp": s, "dp": 2 * x + other}
-    chip = s * pairs + x
+    n_pl = n_y * pairs
+    plane = y * pairs + x
+    chip = plane * n_z + z
+    own_pl = max(1, n_own // n_z)
+    full = own_pl == n_pl
 
     def rc(src, dst, ssem, rsem, dev):
         return pltpu.make_async_remote_copy(
@@ -110,30 +114,33 @@
     def at_z(o):
         return {"sp": (z + o) % n_z * n_y + y, "dp": dpi}
 
-    def at_chip(o):
-        to = (chip + o) % n_chips
-        return {"sp": to // pairs, "dp": 2 * (to % pairs) + c}
+    def at_plane(o):
+        to = (plane + o) % n_pl
+        return {"sp": z * n_y + to // pairs, "dp": 2 * (to % pairs) + c}
 
     def w_own():
         return rc(wfull.at[dpi], wfull.at[dpi], wown_s, wown_r, mate)
 
     def w_x(k, h):
         block = wfull.at[dpi, y, zp, h]
-        return rc(block, block, wx_s.at[k, h], wx_r.at[k, h], at_x(k))
+        return rc(block, block, wx_s.at[k - 1], wx_r.at[k - 1, h], at_x(k))
 
     def w_y(k, h, o):
         block = wfull.at[2 * down(k) + c, y, zp, h]
-        return rc(block, block, wy_s.at[k, h, o], wy_r.at[k, h, o], at_y(o))
+        return rc(block, block, wy_s.at[k - 1, o - 1], wy_r.at[k - 1, h, o - 1], at_y(o))
 
     def w_z(k, h, o):
         a = (y + o) % n_y
         block = wfull.at[2 * down(k) + c, a, zp, h]
         to = {"sp": (z + 1 - 2 * zp) * n_y + y, "dp": dpi}
-        return rc(block, block, wz_s.at[k, h, o], wz_r.at[k, h, o], to)
+        return rc(block, block, wz_s.at[k - 1], wz_r.at[k - 1, h, o], to)
 
     def w_fw(k, a, zz, h):
         block = wfull.at[2 * down(k) + c, a, zz, h]
-        return rc(block, block, wfw_s.at[k, a, zz, h], wfw_r.at[k, a, zz, h], mate)
+        return rc(block, block, wfw_s.at[k - 1], wfw_r.at[k - 1], mate)
+
+    def sized(ref, ssem, rsem):
+        return rc(ref, ref, ssem, rsem, mate)
 
     units = [(q, 0, span) for q in range(gpc - 1)]
     units += [(gpc - 1, 0, span // 2), (gpc - 1, span // 2, span // 2)]
@@ -143,14 +150,14 @@
         return (2 * xx + cc) * gpc + q
 
     def t_core(k, q):
-        return rc(part.at[gid(up(k), other, q)], rcore.at[k, q], core_s.at[k, q], core_r.at[k, q], mate)
+        return rc(part.at[gid(up(k), other, q)], rcore.at[k, q], core_s.at[k], core_r.at[k, q], mate)
 
     def t_x(k, n, a):
         q, lo, size = units[n]
         at = pl.ds(lo, size)
         return rc(
             part.at[gid(up(k), c, q), a, :, at], rx.at[k - 1, q, a, :, at],
-            xs_s.at[k, n, a], xs_r.at[k, n, a], at_x(k),
+            xs_s.at[k - 1], xs_r.at[k - 1, n, a], at_x(k),
         )
 
     def t_yr(n, o, b):
@@ -158,20 +165,15 @@
         at = pl.ds(lo, size)
         return rc(
             part.at[gid(x, c, q), (y + o) % n_y, b, at], ry.at[q, o - 1, b, at],
-            yr_s.at[n, o], yr_r.at[n, o, b], at_y(o),
+            yr_s.at[o - 1], yr_r.at[n, o - 1, b], at_y(o),
         )
-
-    def all_yr(n, o):
-        q, lo, size = units[n]
-        block = part.at[gid(x, c, q), (y + o) % n_y, :, pl.ds(lo, size)]
-        return rc(block, block, yr_s.at[n, o], yr_r.at[n, o, 0], mate)
 
     def z_send(n, b, slot, dst_slot, to):
         q, lo, size = units[n]
         at = pl.ds(lo, size)
         return rc(
             part.at[gid(x, c, q), y, b, at], rz.at[q, dst_slot, at],
-            zr_s.at[n, slot], zr_r.at[n, slot], to,
+            zr_s, zr_r.at[n, slot - 1], to,
         )
 
     to_pair = {"sp": (z + 1 - 2 * zp) * n_y + y, "dp": dpi}
@@ -192,46 +194,62 @@
         return rc(block, block, ssem, rsem, to)
 
     def t_za(n, o):
-        return gathered(n, z, za_s.at[n, o], za_r.at[n, o], at_z(o))
+        return gathered(n, z, za_s, za_r.at[n, o - 1], at_z(o))
 
     def t_ap(n, m):
-        return gathered(n, (z + 2 * m) % n_z, za_s.at[n, 2 * m + 1], za_r.at[n, 2 * m + 1], to_pair)
+        return gathered(n, (z + 2 * m) % n_z, za_s, za_r.at[n, 2 * m], to_pair)
 
     def t_ya(n, o, b):
-        return gathered(n, b, ya_s.at[n, o], ya_r.at[n, o], at_y(o))
+        return gathered(n, b, ya_s.at[o - 1], ya_r.at[n, o - 1], at_y(o))
 
     def all_ya(n, o):
         q, lo, size = units[n]
         block = ag.at[q, y, :, pl.ds(lo, size)]
-        return rc(block, block, ya_s.at[n, o], ya_r.at[n, o], mate)
+        return sized(block, ya_s.at[o - 1], ya_r.at[n, o - 1])
 
     def t_sa(k, j):
         chunk = 2 * down(k) + j
-        return rc(sbuf.at[chunk, other], acore.at[chunk], sa_s.at[chunk], sa_r.at[chunk], mate)
-
-    def t_sb(chunk, o):
-        to = (chip + o) % n_chips
-        return rc(sbuf.at[chunk, c, to % n_own], srecv.at[chunk, o - 1], sb_s.at[chunk], sb_r.at[chunk], at_chip(o))
-
-    def t_sc(j, o):
-        block = fin.at[j, c, chip % n_own]
-        return rc(block, block, sc_s.at[j], sc_r.at[j], at_chip(o))
-
-    def all_sb(chunk):
-        return rc(srecv.at[chunk], srecv.at[chunk], sb_s.at[chunk], sb_r.at[chunk], mate)
-
-    def all_sc(j):
-        block = fin.at[j, c, pl.ds(0, n_own - 1)]
-        return rc(block, block, sc_s.at[j], sc_r.at[j], mate)
+        return rc(sbuf.at[chunk, other], acore.at[chunk], sa_s, sa_r.at[chunk], mate)
+
+    def pieces(to):
+        return pl.ds(to % own_pl * n_z, n_z)
+
+    def t_s1(chunk, o):
+        to = (plane + o) % n_pl
+        return rc(sbuf.at[chunk, c, pieces(to)], s1r.at[chunk, o - 1], s1_s.at[chunk], s1_r.at[chunk], at_plane(o))
+
+    def t_s2(chunk, o):
+        to = plane % own_pl * n_z + (z + o) % n_z
+        return rc(sbuf.at[chunk, c, to], s2r.at[chunk, o - 1], s2_s.at[chunk], s2_r.at[chunk], at_z(o))
+
+    def t_s3(j, o):
+        block = fin.at[j, c, plane % own_pl * n_z + z]
+        return rc(block, block, s3_s.at[j], s3_r.at[j], at_z(o))
+
+    def t_s4(j, o):
+        block = fin.at[j, c, pieces(plane)]
+        return rc(block, block, s4_s.at[j], s4_r.at[j], at_plane(o))
 
     def t_sd(j):
         return rc(fin.at[j, c], fin.at[j, c], sd_s.at[j], sd_r.at[j], mate)
 
+    def all_s1(chunk):
+        return sized(s1r.at[chunk], s1_s.at[chunk], s1_r.at[chunk])
+
+    def all_s2(chunk):
+        return sized(s2r.at[chunk], s2_s.at[chunk], s2_r.at[chunk])
+
+    def all_s3(j):
+        return sized(fin.at[j, c, pl.ds(0, n_z - 1)], s3_s.at[j], s3_r.at[j])
+
+    def all_s4(j):
+        return sized(fin.at[j, c, pl.ds(0, (n_pl - 1) * n_z)], s4_s.at[j], s4_r.at[j])
+
     def owner(t, fn):
-        if n_own == n_chips:
+        if full:
             fn()
         else:
-            pl.when(t < n_own)(fn)
+            pl.when(t < own_pl)(fn)
 
     row = lax.broadcasted_iota(jnp.int32, (span, span), 0)
     col = lax.broadcasted_iota(jnp.int32, (span, span), 1)
@@ -266,9 +284,10 @@
                 load.start()
     barrier = pltpu.get_barrier_semaphore()
     pl.semaphore_signal(barrier, inc=1, device_id=mate, device_id_type=pl.DeviceIdType.MESH)
-    each(1, n_chips, lambda o: pl.semaphore_signal(
-        barrier, inc=1, device_id=at_chip(o), device_id_type=pl.DeviceIdType.MESH,
-    ))
+    for o in range(1, n_pl):
+        pl.semaphore_signal(barrier, inc=1, device_id=at_plane(o), device_id_type=pl.DeviceIdType.MESH)
+    for o in range(1, n_z):
+        pl.semaphore_signal(barrier, inc=1, device_id=at_z(o), device_id_type=pl.DeviceIdType.MESH)
 
     def lanes(g):
         return pl.ds(pl.multiple_of(g * chans, chans), chans)
@@ -340,10 +359,7 @@
             w_fw(k, (y + o) % n_y, 1 - zp, h).start()
 
     def w_ready(k):
-        for h in range(2):
-            for zz in range(2):
-                for a in range(n_y):
-                    w_fw(k, a, zz, h).wait_recv()
+        sized(wfull.at[2 * down(k) + other], wfw_s.at[k - 1], wfw_r.at[k - 1]).wait_recv()
 
     def yr_start(n):
         q, lo, size = units[n]
@@ -487,7 +503,7 @@
             forward_block(0, 4 * b + n)
     each(0, nb // 4, first_blocks)
     load_w.wait()
-    pl.semaphore_wait(barrier, n_chips)
+    pl.semaphore_wait(barrier, n_pl + n_z - 1)
     for h in range(2):
         for k in range(1, pairs):
             w_x(k, h).start()
@@ -514,33 +530,60 @@
     def sa_start(k, j):
         t_sa(k, j).start()
 
-    def sb_start(k, j):
+    def s1_start(k, j):
         t_sa(k, j).wait_recv()
         chunk = 2 * down(k) + j
 
         def one(p):
             sbuf[chunk, c, p] = (sbuf[chunk, c, p].astype(F32) + acore[chunk, p].astype(F32)).astype(BF16)
         each(0, n_own, one)
-        each(1, n_chips, lambda o: owner((chip + o) % n_chips, lambda: t_sb(chunk, o).start()))
-
-    def sc_start(j):
+        for o in range(1, n_pl):
+            owner((plane + o) % n_pl, lambda o=o: t_s1(chunk, o).start())
+
+    def s2_start(j):
         def mine():
             for xx in range(pairs):
                 chunk = 2 * xx + j
-                all_sb(chunk).wait_recv()
-                total = lax.fori_loop(
-                    1, n_chips, lambda o, a: a + srecv[chunk, o - 1].astype(F32),
-                    sbuf[chunk, c, chip % n_own].astype(F32),
-                )
-                fin[j, c, chip % n_own, xx] = total.astype(BF16)
-            each(1, n_chips, lambda o: t_sc(j, o).start())
-        owner(chip, mine)
+                all_s1(chunk).wait_recv()
+
+                def one(n, chunk=chunk):
+                    p = plane % own_pl * n_z + n
+                    total = sbuf[chunk, c, p].astype(F32)
+                    for o in range(1, n_pl):
+                        total = total + s1r[chunk, o - 1, n].astype(F32)
+                    sbuf[chunk, c, p] = total.astype(BF16)
+                each(0, n_z, one)
+                for o in range(1, n_z):
+                    t_s2(chunk, o).start()
+        owner(plane, mine)
+
+    def s3_start(j):
+        def mine():
+            p = plane % own_pl * n_z + z
+            for xx in range(pairs):
+                chunk = 2 * xx + j
+                all_s2(chunk).wait_recv()
+                total = sbuf[chunk, c, p].astype(F32)
+                for o in range(1, n_z):
+                    total = total + s2r[chunk, o - 1].astype(F32)
+                fin[j, c, p, xx] = total.astype(BF16)
+            for o in range(1, n_z):
+                t_s3(j, o).start()
+        owner(plane, mine)
+
+    def s4_start(j):
+        def mine():
+            all_s3(j).wait_recv()
+            for o in range(1, n_pl):
+                t_s4(j, o).start()
+        owner(plane, mine)
 
     def sd_start(j):
-        if n_own == n_chips:
-            all_sc(j).wait_recv()
+        if full:
+            all_s4(j).wait_recv()
         else:
-            each(1, n_chips, lambda o: owner((chip + n_chips - o) % n_chips, lambda: t_sc(j, o).wait_recv()))
+            for o in range(1, n_pl):
+                owner((plane + n_pl - o) % n_pl, lambda o=o: t_s4(j, o).wait_recv())
         t_sd(j).start()
 
     fwd_0, fwd_us, bwd_0, bwd_us, pause_at, pause_us = TIMES
@@ -586,11 +629,10 @@
     for turn in range(n_dp):
         end = 2 * (turn + 1) * per_chunk
         put_slot(end - 1, 0.0, sa_start, turn // 2, turn % 2)
-        put_slot(end, 0.5 if end < n_slots else T_END[0], sb_start, turn // 2, turn % 2)
-    put(T_END[1], sc_start, 0)
-    put(T_END[2], sc_start, 1)
-    put(T_END[3], sd_start, 0)
-    put(T_END[4], sd_start, 1)
+        put_slot(end, 0.5 if end < n_slots else T_END[0], s1_start, turn // 2, turn % 2)
+    for j in range(2):
+        for fn, time in zip((s2_start, s3_start, s4_start, sd_start), T_END[1 + 4 * j : 5 + 4 * j]):
+            put(time, fn, j)
 
     def sd_done():
         for j in range(2):
@@ -731,47 +773,31 @@
 
     w_own().wait_send()
     for k in range(1, pairs):
-        for h in range(2):
-            w_x(k, h).wait_send()
-            for o in range(n_y):
-                w_z(k, h, o).wait_send()
-            for o in range(1, n_y):
-                w_y(k, h, o).wait_send()
-        for h in range(2):
-            for zz in range(2):
-                each(0, n_y, lambda a: w_fw(k, a, zz, h).wait_send())
-        for n in range(len(units)):
-            each(0, n_y, lambda a: t_x(k, n, a).wait_send())
+        mine = wfull.at[2 * down(k) + c]
+        sized(wfull.at[dpi, y, zp], wx_s.at[k - 1], wx_r.at[k - 1, 0]).wait_send()
+        for o in range(1, n_y):
+            sized(mine.at[y, zp], wy_s.at[k - 1, o - 1], wy_r.at[k - 1, 0, o - 1]).wait_send()
+        sized(mine.at[:, zp], wz_s.at[k - 1], wz_r.at[k - 1, 0, 0]).wait_send()
+        sized(mine, wfw_s.at[k - 1], wfw_r.at[k - 1]).wait_send()
+        sized(rx.at[k - 1], xs_s.at[k - 1], xs_r.at[k - 1, 0, 0]).wait_send()
     for k in range(pairs):
-        each(0, gpc, lambda q: t_core(k, q).wait_send())
-
-    for n in range(len(units)):
-        for o in range(1, n_y):
-            all_yr(n, o).wait_send()
-            all_ya(n, o).wait_send()
-        if len(T_UNIT[n + 5 - len(units)]) == 5:
-            for o in range(1, n_z):
-                t_zr(n, o).wait_send()
-                t_za(n, o).wait_send()
+        sized(rcore.at[k], core_s.at[k], core_r.at[k, 0]).wait_send()
+    for o in range(1, n_y):
+        sized(ry.at[:, o - 1], yr_s.at[o - 1], yr_r.at[0, o - 1, 0]).wait_send()
+        sized(ry.at[:, o - 1], ya_s.at[o - 1], ya_r.at[0, o - 1]).wait_send()
+    sized(rz, zr_s, zr_r.at[0, 0]).wait_send()
+    sized(rz, za_s, za_r.at[0, 0]).wait_send()
+    sized(acore, sa_s, sa_r.at[0]).wait_send()
+    for chunk in range(n_dp):
+        if full:
+            all_s1(chunk).wait_send()
         else:
-            for m in range(half_z):
-                t_zp(n, m).wait_send()
-                t_ap(n, m).wait_send()
-            for m in range(1, half_z):
-                t_zc(n, m).wait_send()
-                t_za(n, 2 * m).wait_send()
-    for k in range(pairs):
-        for j in range(2):
-            t_sa(k, j).wait_send()
-    if n_own == n_chips:
-        each(0, n_dp, lambda chunk: all_sb(chunk).wait_send())
-    else:
-        each(0, n_dp, lambda chunk: each(1, n_chips, lambda o: owner((chip + o) % n_chips, lambda: t_sb(chunk, o).wait_send())))
+            for o in range(1, n_pl):
+                owner((plane + o) % n_pl, lambda o=o: t_s1(chunk, o).wait_send())
+        owner(plane, lambda: all_s2(chunk).wait_send())
     for j in range(2):
-        if n_own == n_chips:
-            all_sc(j).wait_send()
-        else:
-            owner(chip, lambda: each(1, n_chips, lambda o: t_sc(j, o).wait_send()))
+        owner(plane, lambda: all_s3(j).wait_send())
+        owner(plane, lambda: [t_s4(j, o).wait_send() for o in range(1, n_pl)] and None) if not full else all_s4(j).wait_send()
         t_sd(j).wait_send()
 
 
@@ -853,21 +879,24 @@
         vm((2, 4, span, chans), F32),
         vm((n_dp, 2, n_own, prow, chans), BF16),
         vm((n_dp, n_own, prow, chans), BF16),
-        vm((n_dp, n_chips - 1, prow, chans), BF16),
+        vm((n_dp, n_y * pairs - 1, n_z, prow, chans), BF16),
+        vm((n_dp, n_z - 1, prow, chans), BF16),
         vm((2, 2, n_own, pairs, prow, chans), BF16),
         dma, dma,
-        dma((pairs, 2)), dma((pairs, 2)),
-        dma((pairs, 2, n_y)), dma((pairs, 2, n_y)),
-        dma((pairs, 2, n_y)), dma((pairs, 2, n_y)),
-        dma((pairs, n_y, 2, 2)), dma((pairs, n_y, 2, 2)),
-        dma((pairs, gpc)), dma((pairs, gpc)),
-        dma((pairs, gpc + 1, n_y)), dma((pairs, gpc + 1, n_y)),
-        dma((gpc + 1, n_y)), dma((gpc + 1, n_y, n_z)),
-        dma((gpc + 1, n_z)), dma((gpc + 1, n_z)),
-        dma((gpc + 1, n_z)), dma((gpc + 1, n_z)),
-        dma((gpc + 1, n_y)), dma((gpc + 1, n_y)),
+        dma((pairs - 1,)), dma((pairs - 1, 2)),
+        dma((pairs - 1, n_y - 1)), dma((pairs - 1, 2, n_y - 1)),
+        dma((pairs - 1,)), dma((pairs - 1, 2, n_y)),
+        dma((pairs - 1,)), dma((pairs - 1,)),
+        dma((pairs,)), dma((pairs, gpc)),
+        dma((pairs - 1,)), dma((pairs - 1, gpc + 1, n_y)),
+        dma((n_y - 1,)), dma((gpc + 1, n_y - 1, n_z)),
+        dma, dma((gpc + 1, n_z - 1)),
+        dma, dma((gpc + 1, n_z - 1)),
+        dma((n_y - 1,)), dma((gpc + 1, n_y - 1)),
+        dma, dma((n_dp,)),
         dma((n_dp,)), dma((n_dp,)),
         dma((n_dp,)), dma((n_dp,)),
+        dma((2,)), dma((2,)),
         dma((2,)), dma((2,)),
         dma((2,)), dma((2,)),
     ]

time: 110 us -> 102 us (0.927)
  Pallas kernels: 109 us -> 101 us
    pallas_call x1, Pallas kernels: 104 us -> 95.5 us  [on_device(): pl.pallas_call(functools.partial(kernel, dims), out_shape=(vm((rows, wide...]
where the time goes in v2:
time: 102 us
  Pallas kernels  101 us (99%)
    pallas_call x1, Pallas kernels, on_device(): pl.pallas_call(functools.partial(kernel, dims), out_shape=(vm((rows, wide...  95.5 us
    pallas_call x1, Pallas kernels, on_device(): pl.pallas_call(functools.partial(finish, (gpc, span, chans, width, n_sp,...  5.55 us

profile of v2, /device:TPU:0, one launch (start us, length us, event | category | flops | bytes accessed | tf_op | source)
XLA Modules:
  0.0 101.7 jit_solution(16900268561877974053)
XLA Ops:
  0.6 95.5 %shard_map.135 = (bf16[1024,2048]{1,0:T(8,128)(2,1)S(1)}, bf16[1024,2048]{1,0:T(8,128)(2,1)S(1)}, bf16[4,8,128,256]{3,2,1,0:T(8,128)(2,1)S(1)}, bf16[2,2,16,2,16,128]{5,4,3,2,1,0:T(8,128)(2,1)S(1)}) custom-call(bf16[1024,2048]{1,0:T(8,128)(2,1)} %bitcast.7, bf16[1024,2048]{1,0:T(8,128)(2,1)} %bitcast.8, bf16[1024,2048]{1,0:T(8,128)(2,1)} %bitcast.9, ...), custom_call_target="tpu_custom_call" | custom-call | tf_op jit(solution)/shard_map/pallas_call | solution.py:905
  96.1 5.5 %shard_map.136 = (bf16[1,1024,2048]{2,1,0:T(8,128)(2,1)}, bf16[1,1024,2048]{2,1,0:T(8,128)(2,1)}, f32[512,2048]{1,0:T(8,128)}, f32[16,128,128]{2,1,0:T(8,128)}, ...) custom-call(bf16[1024,2048]{1,0:T(8,128)(2,1)S(1)} %get-tuple-element.11.gu_ref, ...), custom_call_target="tpu_custom_call" | custom-call | tf_op jit(solution)/shard_map/pallas_call | solution.py:924
